TPU v7x, 32 devices: a whole 2x2x4 slice. The times are simulated.
32 devices in a mesh: fs: 8 (over z, y), tp: 4 (over x, core).
Axes of the slice: x: 2, y: 2, z: 4, core: 2. Of those that a mesh axis runs over, the one named last changes fastest.
Arguments:
- tokens: bfloat16 [8192, 2048], P('fs', 'tp'), may hold values from -6 to 6
- mixer_gain: float32 [2048], replicated, may hold values from 0.1 to 1.9
- conv_taps: bfloat16 [3, 1024], replicated, may hold values from -3.5 to 3.5
- outer_weight: bfloat16 [2048, 1024], P('fs', 'tp'), may hold values from -0.125 to 0.125
- inner_weight: bfloat16 [2048, 1024], P('fs', 'tp'), may hold values from -0.125 to 0.125
- value_weight: bfloat16 [2048, 1024], P('fs', 'tp'), may hold values from -0.125 to 0.125
- merge_weight: bfloat16 [1024, 2048], P('tp', 'fs'), may hold values from -0.25 to 0.25
- merge_gain: float32 [2048], replicated, may hold values from 0.1 to 1.9
- channel_gain: float32 [2048], replicated, may hold values from 0.1 to 1.9
- gate_weight: bfloat16 [2048, 5632], P('fs', 'tp'), may hold values from -0.125 to 0.125
- up_weight: bfloat16 [2048, 5632], P('fs', 'tp'), may hold values from -0.125 to 0.125
- down_weight: bfloat16 [5632, 2048], P('tp', 'fs'), may hold values from -0.109375 to 0.109375
- output_gain: float32 [2048], replicated, may hold values from 0.1 to 1.9
Outputs:
- layer_out: bfloat16 [8192, 2048], P('fs', 'tp')
All inputs are finite; a program needn't handle non-finite values.
Results may differ from a plain program's by a relative error of at most 0.018.
Values may be sent and summed in bfloat16 or wider, within the bound.
A program may use at most 128 MiB of HBM per device.

v0:
```python
import jax
import jax.numpy as jnp
from jax import lax
from jax.sharding import PartitionSpec as P

HEAD_DIM = 128


EPS = 1e-06


def normalize(values):
    floats = values.astype(jnp.float32)
    return floats * lax.rsqrt(jnp.mean(floats * floats, axis=-1, keepdims=True) + EPS)


def rounded_term(partial_value):
    return lax.optimization_barrier(partial_value.astype(jnp.bfloat16)).astype(jnp.float32)


def finish_scatter(summed, residual, gain_row, squares):
    floats = summed.astype(jnp.float32)
    columns = floats.shape[1]
    factor = lax.rsqrt(squares / (columns * lax.axis_size("tp")) + EPS)
    own_gain = lax.dynamic_slice_in_dim(gain_row, lax.axis_index("tp") * columns, columns)
    return (residual.astype(jnp.float32) + floats * factor[:, None] * own_gain).astype(jnp.bfloat16)


def shards(
    tokens,
    mixer_gain,
    conv_taps,
    outer_weight,
    inner_weight,
    value_weight,
    merge_weight,
    merge_gain,
    channel_gain,
    gate_weight,
    up_weight,
    down_weight,
    output_gain,
):
    whole_tokens = lax.all_gather(tokens, "tp", axis=1, tiled=True)
    normed = (normalize(whole_tokens) * mixer_gain).astype(jnp.bfloat16)
    length = normed.shape[0]
    channels = outer_weight.shape[1]
    full_outer, full_inner, full_value = (
        lax.all_gather(outer_weight, "fs", axis=0, tiled=True),
        lax.all_gather(inner_weight, "fs", axis=0, tiled=True),
        lax.all_gather(value_weight, "fs", axis=0, tiled=True),
    )
    outer = jnp.dot(normed, full_outer, preferred_element_type=jnp.float32)
    inner = jnp.dot(normed, full_inner, preferred_element_type=jnp.float32)
    value = jnp.dot(normed, full_value, preferred_element_type=jnp.float32)
    own_taps = lax.dynamic_slice_in_dim(
        conv_taps, lax.axis_index("tp") * channels, channels, 1
    ).astype(jnp.float32)
    signal = inner * value
    padded = jnp.pad(signal, ((2, 0), (0, 0)))
    conv = (
        own_taps[0] * padded[:length]
        + own_taps[1] * padded[1 : length + 1]
        + own_taps[2] * padded[2:]
    )
    gated = (outer * conv).reshape(length, channels // HEAD_DIM, HEAD_DIM)
    mixed = normalize(gated).reshape(length, channels).astype(jnp.bfloat16)
    merged_part = jnp.dot(
        mixed,
        lax.all_gather(merge_weight, "fs", axis=1, tiled=True),
        preferred_element_type=jnp.float32,
    )
    merged = lax.psum(rounded_term(merged_part).astype(jnp.bfloat16), "tp")
    first_full = (whole_tokens.astype(jnp.float32) + normalize(merged) * merge_gain).astype(
        jnp.bfloat16
    )
    width = tokens.shape[1]
    first = lax.dynamic_slice_in_dim(first_full, lax.axis_index("tp") * width, width, 1)
    normed2 = (normalize(first_full) * channel_gain).astype(jnp.bfloat16)
    full_gate, full_up = (
        lax.all_gather(gate_weight, "fs", axis=0, tiled=True),
        lax.all_gather(up_weight, "fs", axis=0, tiled=True),
    )
    gate = jnp.dot(normed2, full_gate, preferred_element_type=jnp.float32)
    upward = jnp.dot(normed2, full_up, preferred_element_type=jnp.float32)
    hidden = (jax.nn.silu(gate) * upward).astype(jnp.bfloat16)
    down_part = jnp.dot(
        hidden,
        lax.all_gather(down_weight, "fs", axis=1, tiled=True),
        preferred_element_type=jnp.float32,
    )
    down = lax.psum_scatter(
        rounded_term(down_part).astype(jnp.bfloat16), "tp", scatter_dimension=1, tiled=True
    )
    down_float = down.astype(jnp.float32)
    down_squares = lax.psum(jnp.sum(down_float * down_float, axis=1), "tp")
    return finish_scatter(down, first, output_gain, down_squares)


def solution(mesh):
    return jax.shard_map(
        shards,
        mesh=mesh,
        in_specs=(
            P("fs", "tp"),
            P(),
            P(),
            P("fs", "tp"),
            P("fs", "tp"),
            P("fs", "tp"),
            P("tp", "fs"),
            P(),
            P(),
            P("fs", "tp"),
            P("fs", "tp"),
            P("tp", "fs"),
            P(),
        ),
        out_specs=P("fs", "tp"),
        check_vma=False,
    )
```

profile of v0, /device:TPU:0, one launch (start us, length us, event | category | flops | bytes accessed | tf_op | source)
XLA Modules:
  0.0 661.4 jit_solution(1043669761443059637)
XLA Ops:
  6.5 0.0 copy-start.2
  6.5 0.0 all-gather.9.cloned.1.call-start
  6.5 0.7 all-gather.9.cloned.1.call-update
  7.3 0.0 all-gather.13.cloned.1.call-start
  7.3 0.7 all-gather.13.cloned.1.call-update
  8.0 0.0 all-gather.15.cloned.1.call-start
  8.1 0.7 all-gather.15.cloned.1.call-update
  8.7 0.0 all-gather.11.cloned.1.call-start
  8.8 0.5 all-gather.11.cloned.1.call-update
  9.3 0.0 all-gather.17.cloned.1.call-start
  9.4 0.5 all-gather.17.cloned.1.call-update
  9.9 0.0 all-reduce.3.cloned.1.call-start
  10.0 0.7 dynamic-slice_convert_fusion
  10.7 35.5 %all-gather.9.cloned.1.call-done = bf16[1024,2048]{1,0:T(8,128)(2,1)} async-done(((bf16[1024,512]{1,0:T(8,128)(2,1)}), bf16[1024,2048]{1,0:T(8,128)(2,1)}) %all-gather.9.cloned.1.call-update) | async-done | bytes 4194320 | tf_op jit(solution)/shard_map/all_gather | solution.py:44
  46.1 3.1 fusion.5
  49.2 39.4 %all-gather.13.cloned.1.call-done = bf16[2048,256]{1,0:T(8,128)(2,1)} async-done(((bf16[256,256]{1,0:T(8,128)(2,1)}), bf16[2048,256]{1,0:T(8,128)(2,1)}) %all-gather.13.cloned.1.call-update) | async-done | bytes 1048592 | tf_op jit(solution)/shard_map/all_gather | solution.py:50
  88.5 0.0 copy-done.2
  88.5 4.0 fusion.22
  92.5 37.2 %all-gather.15.cloned.1.call-done = bf16[2048,256]{1,0:T(8,128)(2,1)} async-done(((bf16[256,256]{1,0:T(8,128)(2,1)}), bf16[2048,256]{1,0:T(8,128)(2,1)}) %all-gather.15.cloned.1.call-update) | async-done | bytes 1048592 | tf_op jit(solution)/shard_map/all_gather | solution.py:51
  129.7 4.0 convolution_multiply_fusion
  133.7 37.0 %all-gather.11.cloned.1.call-done = bf16[2048,256]{1,0:T(8,128)(2,1)} async-done(((bf16[256,256]{1,0:T(8,128)(2,1)}), bf16[2048,256]{1,0:T(8,128)(2,1)}) %all-gather.11.cloned.1.call-update) | async-done | bytes 1048592 | tf_op jit(solution)/shard_map/all_gather | solution.py:49
  170.7 4.4 bitcast_reduce_fusion
  175.1 0.1 fusion.20
  175.2 35.5 %all-gather.17.cloned.1.call-done = bf16[256,2048]{1,0:T(8,128)(2,1)} async-done(((bf16[256,256]{1,0:T(8,128)(2,1)}), bf16[256,2048]{1,0:T(8,128)(2,1)}) %all-gather.17.cloned.1.call-update) | async-done | bytes 1048592 | tf_op jit(solution)/shard_map/all_gather | solution.py:70
  210.7 4.6 convolution_convert_fusion.1
  215.3 0.0 copy-start.1
  215.3 0.0 all-reduce.3.cloned.1.call-update
  215.3 0.0 all-gather.19.cloned.1.call-start
  215.4 0.7 all-gather.19.cloned.1.call-update
  216.1 0.0 all-gather.21.cloned.1.call-start
  216.1 0.7 all-gather.21.cloned.1.call-update
  216.8 0.0 all-gather.23.cloned.1.call-start
  216.9 0.7 all-gather.23.cloned.1.call-update
  217.5 0.2 reduce-scatter.2.cloned.1.call-start
  217.8 82.2 %all-reduce.3.cloned.1.call-done = bf16[1024,2048]{1,0:T(8,128)(2,1)} async-done(((bf16[1024,2048]{1,0:T(8,128)(2,1)}), bf16[1024,2048]{1,0:T(8,128)(2,1)}) %all-reduce.3.cloned.1.call-update) | async-done | bytes 4194320 | tf_op jit(solution)/shard_map/psum | solution.py:73
  300.0 0.0 copy-start
  300.0 3.2 fusion
  303.2 0.0 copy-done.1
  303.2 0.2 copy-done
  303.4 0.0 copy-start.3
  303.4 5.3 fusion.2
  308.8 85.9 %all-gather.19.cloned.1.call-done = bf16[2048,1408]{1,0:T(8,128)(2,1)} async-done(((bf16[256,1408]{1,0:T(8,128)(2,1)}), bf16[2048,1408]{1,0:T(8,128)(2,1)}) %all-gather.19.cloned.1.call-update) | async-done | bytes 5767184 | tf_op jit(solution)/shard_map/all_gather | solution.py:81
  394.6 0.0 copy-done.3
  394.6 12.0 %fusion.14 = f32[1024,1408]{1,0:T(8,128)} fusion(bf16[2048,1408]{1,0:T(8,128)(2,1)} %all-gather.19.cloned.1.call-done, bf16[1024,2048]{1,0:T(8,128)(2,1)} %get-tuple-element.6, f32[2048]{0:T(1024)S(1)} %copy-done.3, f32[1024]{0:T(1024)S(1)} %add_rsqrt_fusion.2), kind=kOutput, calls=%fused_computation.27 | convolution fusion | flops 5913968640 | bytes 15740928 | tf_op jit(solution)/shard_map/dot_general | solution.py:84
  406.6 80.7 %all-gather.21.cloned.1.call-done = bf16[2048,1408]{1,0:T(8,128)(2,1)} async-done(((bf16[256,1408]{1,0:T(8,128)(2,1)}), bf16[2048,1408]{1,0:T(8,128)(2,1)}) %all-gather.21.cloned.1.call-update) | async-done | bytes 5767184 | tf_op jit(solution)/shard_map/all_gather | solution.py:82
  487.3 93.4 %all-gather.23.cloned.1.call-done = bf16[1408,2048]{1,0:T(8,128)(2,1)} async-done(((bf16[1408,256]{1,0:T(8,128)(2,1)}), bf16[1408,2048]{1,0:T(8,128)(2,1)}) %all-gather.23.cloned.1.call-update) | async-done | bytes 5767184 | tf_op jit(solution)/shard_map/all_gather | solution.py:89
  580.7 20.8 %convolution_convert_fusion = bf16[1024,2048]{1,0:T(8,128)(2,1)} fusion(bf16[1408,2048]{1,0:T(8,128)(2,1)} %all-gather.23.cloned.1.call-done, f32[1024,1408]{1,0:T(8,128)} %fusion.14, bf16[2048,1408]{1,0:T(8,128)(2,1)} %all-gather.21.cloned.1.call-done, bf16[1024,2048]{1,0:T(8,128)(2,1)} %get-tuple-element.6, f32[2048]{0:T(1024)S(1)} %copy-done.3, ...), kind=kOutput, calls=%fused_computation.17 | convolution fusion | flops 11830296576 | bytes 25702400 | tf_op jit(solution)/shard_map/dot_general | solution.py:87
  601.6 0.0 reduce-scatter.2.cloned.1.call-update
  601.6 0.8 dynamic_slice.11
  602.3 42.0 %reduce-scatter.2.cloned.1.call-done = bf16[1024,512]{1,0:T(8,128)(2,1)} async-done(((bf16[1024,2048]{1,0:T(8,128)(2,1)}), bf16[1024,512]{1,0:T(8,128)(2,1)}) %reduce-scatter.2.cloned.1.call-update) | async-done | bytes 1048592 | tf_op jit(solution)/shard_map/reduce_scatter | solution.py:92
  644.3 1.5 fusion.9
  645.8 5.8 psum.15
  651.6 3.0 fusion.12
  (6 shorter events, 0.0 us)
Async XLA Ops:
  6.5 82.0 %copy-start.2 = (f32[2048]{0:T(1024)S(1)}, f32[2048]{0:T(1024)}, u32[]{:S(2)}) copy-start(f32[2048]{0:T(1024)} %param.14) | copy-start | bytes 24580
  6.5 39.6 %all-gather.9.cloned.1.call-start = ((), (), s32[]{:S(2)}) async-start(), calls=%async_computation.1 | async-start | bytes 5242880 | tf_op jit(solution)/shard_map/all_gather | solution.py:44
  7.3 81.3 %all-gather.13.cloned.1.call-start = ((), (), s32[]{:S(2)}) async-start(), calls=%async_computation.3 | async-start | bytes 1179648 | tf_op jit(solution)/shard_map/all_gather | solution.py:50
  8.0 121.7 %all-gather.15.cloned.1.call-start = ((), (), s32[]{:S(2)}) async-start(), calls=%async_computation.4 | async-start | bytes 1179648 | tf_op jit(solution)/shard_map/all_gather | solution.py:51
  8.7 162.0 %all-gather.11.cloned.1.call-start = ((), (), s32[]{:S(2)}) async-start(), calls=%async_computation.2 | async-start | bytes 1179648 | tf_op jit(solution)/shard_map/all_gather | solution.py:49
  9.3 201.4 %all-gather.17.cloned.1.call-start = ((), (), s32[]{:S(2)}) async-start(), calls=%async_computation.5 | async-start | bytes 1179648 | tf_op jit(solution)/shard_map/all_gather | solution.py:70
  9.9 290.1 %all-reduce.3.cloned.1.call-start = ((), (), s32[]{:S(2)}) async-start(), calls=%async_computation.6 | async-start | bytes 8388608 | tf_op jit(solution)/shard_map/psum | solution.py:73
  215.3 87.9 %copy-start.1 = (f32[2048]{0:T(1024)S(1)}, f32[2048]{0:T(1024)}, u32[]{:S(2)}) copy-start(f32[2048]{0:T(1024)} %param.20) | copy-start | bytes 24580
  215.3 179.3 %all-gather.19.cloned.1.call-start = ((), (), s32[]{:S(2)}) async-start(), calls=%async_computation.7 | async-start | bytes 6488064 | tf_op jit(solution)/shard_map/all_gather | solution.py:81
  216.1 271.3 %all-gather.21.cloned.1.call-start = ((), (), s32[]{:S(2)}) async-start(), calls=%async_computation.8 | async-start | bytes 6488064 | tf_op jit(solution)/shard_map/all_gather | solution.py:82
  216.8 363.9 %all-gather.23.cloned.1.call-start = ((), (), s32[]{:S(2)}) async-start(), calls=%async_computation.9 | async-start | bytes 6488064 | tf_op jit(solution)/shard_map/all_gather | solution.py:89
  217.5 426.8 %reduce-scatter.2.cloned.1.call-start = ((), (), s32[]{:S(2)}) async-start(), calls=%async_computation.10 | async-start | bytes 5242880 | tf_op jit(solution)/shard_map/reduce_scatter | solution.py:92
  300.0 3.4 copy-start
  303.4 91.2 %copy-start.3 = (f32[2048]{0:T(1024)S(1)}, f32[2048]{0:T(1024)}, u32[]{:S(2)}) copy-start(f32[2048]{0:T(1024)} %param.21) | copy-start | bytes 24580
Sparse Core Ops, SparseCore 0:
  8.9 37.1 all-gather.8
  48.2 40.2 all-gather.12
  90.7 38.9 all-gather.14
  131.7 38.9 all-gather.10
  172.6 38.0 all-gather.16
  215.4 84.4 all-reduce.2
  302.1 92.4 all-gather.18
  396.8 90.4 all-gather.20
  489.4 91.2 all-gather.22
  601.7 42.5 reduce-scatter.1
where the time goes:
time: 662 us; the launch traced here: 661 us
  waiting for transfers between devices  574 us (87%)
  matrix products  49.7 us (8%)
  other arithmetic  16.9 us (3%)
  between operations  13.6 us (2%)
    all_gather x1, waiting for transfers between devices, shards(): lax.all_gather(down_weight, 'fs', axis=1, tiled=True)  93.4 us
    all_gather x1, waiting for transfers between devices, shards(): lax.all_gather(gate_weight, 'fs', axis=0, tiled=True)  85.9 us
    psum x1, waiting for transfers between devices, shards(): merged = lax.psum(rounded_term(merged_part).astype(jnp.bfloat16), 'tp')  82.2 us
    all_gather x1, waiting for transfers between devices, shards(): lax.all_gather(up_weight, 'fs', axis=0, tiled=True)  80.7 us
    reduce_scatter x1, waiting for transfers between devices, shards(): lax.psum_scatter(rounded_term(down_part).astype(jnp.bfloat16), 'tp', scat...  42 us
    all_gather x1, waiting for transfers between devices, shards(): lax.all_gather(inner_weight, 'fs', axis=0, tiled=True)  39.4 us
    all_gather x1, waiting for transfers between devices, shards(): lax.all_gather(value_weight, 'fs', axis=0, tiled=True)  37.2 us
    all_gather x1, waiting for transfers between devices, shards(): lax.all_gather(outer_weight, 'fs', axis=0, tiled=True)  37 us
  transfers between devices with their start and end apart: 10, of which 10 were waited for; matrix products, arithmetic and copies ran while one was open for 6% of the time, Pallas kernels for 0%

commit v1 on v0

v1 whole, which is shorter than its diff:
```python
import jax
import jax.numpy as jnp
from jax import lax
from jax.experimental import pallas as pl
from jax.experimental.pallas import tpu as pltpu
from jax.sharding import PartitionSpec as P

HEAD_DIM = 128
EPS = 1e-06
MESH = pl.DeviceIdType.MESH
F32 = jnp.float32
BF16 = jnp.bfloat16
MIX, FEED, DOWN = (0, 1, 2, 3), (4, 5), (6, 7)


def layer_kernel(
    n, nt, tokens, mixer_gain, taps, outer_w, inner_w, value_w, merge_w, merge_gain,
    channel_gain, gate_w, up_w, down_w,
    down_out, first_out,
    toks, nrm, full_outer, full_inner, full_value, full_merge, full_gate, full_up, full_down,
    outer_s, sig, mixed, part, mrecv, msum, merged, hidden, drecv,
    ring_send, ring_recv, tok_send, tok_recv, rs_send, rs_recv, ag_send, ag_recv, dn_send, dn_recv,
):
    f, t = lax.axis_index("fs"), lax.axis_index("tp")
    half = n // 2
    odd = lax.rem(f, 2)
    pos = (1 - odd) * (f // 2) + odd * (n - 1 - f // 2)
    length, width = tokens.shape
    blk, channels = outer_w.shape
    cols = merge_w.shape[1]
    bps = n // nt
    depth = width * nt
    tile = min(256, length)
    tiles = length // tile

    def owner(p):
        q = lax.rem(p + 2 * n, n)
        high = q // half
        return (1 - high) * (2 * q) + high * (2 * (n - 1 - q) + 1)

    right, left = owner(pos + 1), owner(pos - 1)
    rowed = {0: (outer_w, full_outer), 1: (inner_w, full_inner), 2: (value_w, full_value),
             4: (gate_w, full_gate), 5: (up_w, full_up)}
    piece_m = channels // 2
    piece_d = down_w.shape[0] // 4

    def own_region(w, d):
        if w in rowed:
            return rowed[w][0].at[pl.ds(d * (blk // 2), blk // 2)]
        if w == 3:
            return merge_w.at[pl.ds(d * piece_m, piece_m)]
        return down_w.at[pl.ds((d * 2 + w - 6) * piece_d, piece_d)]

    def region(w, d, p):
        i = owner(p)
        if w in rowed:
            start = pl.multiple_of(i * blk + d * (blk // 2), blk // 2)
            return rowed[w][1].at[pl.ds(start, blk // 2)]
        if w == 3:
            return full_merge.at[i, pl.ds(d * piece_m, piece_m)]
        return full_down.at[i, pl.ds((d * 2 + w - 6) * piece_d, piece_d)]

    def ring_copy(w, d, s, first=False):
        p = pos - s if d == 0 else pos + s
        dst = region(w, d, p)
        return pltpu.make_async_remote_copy(
            src_ref=own_region(w, d) if first else dst,
            dst_ref=dst,
            send_sem=ring_send.at[d, w],
            recv_sem=ring_recv.at[d, w, s],
            device_id={"fs": right if d == 0 else left},
            device_id_type=MESH,
        )

    def ring_arrive(w, d, s):
        got = region(w, d, pos - 1 - s if d == 0 else pos + 1 + s)
        pltpu.make_async_remote_copy(
            src_ref=got, dst_ref=got, send_sem=ring_send.at[d, w],
            recv_sem=ring_recv.at[d, w, s],
            device_id={"fs": right if d == 0 else left}, device_id_type=MESH,
        ).wait_recv()

    def ring_open(ws):
        for w in ws:
            for d in (0, 1):
                ring_copy(w, d, 0, True).start()

    def pump(ws, s):
        for w in ws:
            for d in (0, 1):
                ring_arrive(w, d, s - 1)
                ring_copy(w, d, s - 1).wait_send()
                ring_copy(w, d, s).start()

    def pumps(ws, low, high):
        lax.fori_loop(low, high, lambda s, c: (pump(ws, s), c)[1], 0)

    def ring_close(ws):
        for w in ws:
            for d in (0, 1):
                ring_arrive(w, d, n - 2)
                ring_copy(w, d, n - 2).wait_send()

    def peer(o):
        return lax.rem(t + o, nt)

    def slab_copy(src, dst, send, recv, o):
        return pltpu.make_async_remote_copy(
            src_ref=src, dst_ref=dst, send_sem=send.at[o - 1], recv_sem=recv.at[o - 1],
            device_id={"tp": peer(o)}, device_id_type=MESH,
        )

    offsets = range(1, nt)

    barrier = pltpu.get_barrier_semaphore()
    for to in ({"fs": left}, {"fs": right}) + tuple({"tp": peer(o)} for o in offsets):
        pl.semaphore_signal(barrier, inc=1, device_id=to, device_id_type=MESH)
    pl.semaphore_wait(barrier, 2 + nt - 1)

    ring_open(MIX)
    for o in offsets:
        slab_copy(tokens, toks.at[t], tok_send, tok_recv, o).start()

    own_rows = pl.ds(pl.multiple_of(f * blk, blk), blk)
    for source, full in rowed.values():
        full[own_rows, :] = source[...]
    full_merge[f] = merge_w[...]
    full_down[f] = down_w[...]
    toks[t] = tokens[...]
    sig[pl.ds(0, 8), :] = jnp.zeros((8, channels), F32)

    pumps(MIX, 1, n - 1)
    ring_open(FEED)
    for o in offsets:
        slab = toks.at[lax.rem(t - o + nt, nt)]
        slab_copy(tokens, slab, tok_send, tok_recv, o).wait()

    def rows_of(i):
        return pl.ds(pl.multiple_of(i * tile, tile), tile)

    def norm_tile(i, c):
        rows = rows_of(i)
        squares = jnp.zeros((tile, 1), F32)
        for j in range(nt):
            x = toks[j, rows, :].astype(F32)
            squares += jnp.sum(x * x, axis=1, keepdims=True)
        factor = lax.rsqrt(squares / depth + EPS)
        for j in range(nt):
            x = toks[j, rows, :].astype(F32)
            nrm[rows, pl.ds(j * width, width)] = (x * factor * mixer_gain[j]).astype(BF16)
        return c

    lax.fori_loop(0, tiles, norm_tile, 0)
    ring_close(MIX)

    def project(i, c):
        rows = rows_of(i)
        x = nrm[rows, :]
        outer_s[rows, :] = jnp.dot(x, full_outer[...], preferred_element_type=F32)
        inner = jnp.dot(x, full_inner[...], preferred_element_type=F32)
        value = jnp.dot(x, full_value[...], preferred_element_type=F32)
        sig[pl.ds(pl.multiple_of(i * tile + 8, 8), tile), :] = inner * value
        return c

    lax.fori_loop(0, tiles, project, 0)
    for i in range(tiles):
        r = i * tile
        conv = (
            taps[0:1, :] * sig[r + 6 : r + 6 + tile, :]
            + taps[1:2, :] * sig[r + 7 : r + 7 + tile, :]
            + taps[2:3, :] * sig[r + 8 : r + 8 + tile, :]
        )
        gated = outer_s[r : r + tile, :] * conv
        for h in range(channels // HEAD_DIM):
            g = gated[:, h * HEAD_DIM : (h + 1) * HEAD_DIM]
            level = lax.rsqrt(jnp.mean(g * g, axis=1, keepdims=True) + EPS)
            mixed[r : r + tile, h * HEAD_DIM : (h + 1) * HEAD_DIM] = (g * level).astype(BF16)

    def merge_block(b, c):
        part[b] = jnp.dot(mixed[...], full_merge[b], preferred_element_type=F32).astype(BF16)
        return c

    lax.fori_loop(0, n, merge_block, 0)

    def part_slab(j):
        return part.at[pl.ds(j * bps, bps)]

    for o in offsets:
        slab_copy(part_slab(peer(o)), mrecv.at[o - 1], rs_send, rs_recv, o).start()
    cut = (2 * (n - 2) + 2) // 3
    pumps(FEED, 1, cut + 1)
    for o in offsets:
        slab_copy(part_slab(peer(o)), mrecv.at[o - 1], rs_send, rs_recv, o).wait()

    def add_tile(received, target):
        def body(i, c):
            rows = rows_of(i)
            for q in range(bps):
                total = part[t * bps + q, rows, :].astype(F32)
                for o in offsets:
                    total += received[o - 1, q, rows, :].astype(F32)
                target[rows, pl.ds(q * cols, cols)] = total.astype(BF16)
            return c

        lax.fori_loop(0, tiles, body, 0)

    add_tile(mrecv, msum)
    for o in offsets:
        slab_copy(msum, merged.at[t], ag_send, ag_recv, o).start()
    merged[t] = msum[...]
    pumps(FEED, cut + 1, n - 1)
    ring_open(DOWN)
    for o in offsets:
        slab = merged.at[lax.rem(t - o + nt, nt)]
        slab_copy(msum, slab, ag_send, ag_recv, o).wait()

    def first_tile(i, c):
        rows = rows_of(i)
        squares = jnp.zeros((tile, 1), F32)
        for j in range(nt):
            x = merged[j, rows, :].astype(F32)
            squares += jnp.sum(x * x, axis=1, keepdims=True)
        factor = lax.rsqrt(squares / depth + EPS)
        squares = jnp.zeros((tile, 1), F32)
        for j in range(nt):
            x = merged[j, rows, :].astype(F32)
            y = (toks[j, rows, :].astype(F32) + x * factor * merge_gain[j]).astype(BF16)
            toks[j, rows, :] = y
            y = y.astype(F32)
            squares += jnp.sum(y * y, axis=1, keepdims=True)
        factor = lax.rsqrt(squares / depth + EPS)
        for j in range(nt):
            y = toks[j, rows, :].astype(F32)
            nrm[rows, pl.ds(j * width, width)] = (y * factor * channel_gain[j]).astype(BF16)
        return c

    lax.fori_loop(0, tiles, first_tile, 0)
    first_out[...] = toks[t]
    ring_close(FEED)

    def feed_tile(i, c):
        rows = rows_of(i)
        x = nrm[rows, :]
        gate = jnp.dot(x, full_gate[...], preferred_element_type=F32)
        upward = jnp.dot(x, full_up[...], preferred_element_type=F32)
        hidden[rows, :] = (gate / (1.0 + jnp.exp(-gate)) * upward).astype(BF16)
        return c

    lax.fori_loop(0, tiles // 2, feed_tile, 0)
    pump(DOWN, 1)
    lax.fori_loop(tiles // 2, tiles, feed_tile, 0)
    pump(DOWN, 2)

    def down_copy(b):
        j = b // bps
        q = lax.rem(b, bps)
        o = lax.rem(j - t + nt, nt)
        return pltpu.make_async_remote_copy(
            src_ref=part.at[b], dst_ref=drecv.at[o - 1, q],
            send_sem=dn_send.at[b], recv_sem=dn_recv.at[o - 1, q],
            device_id={"tp": j}, device_id_type=MESH,
        )

    def down_block(k):
        b = owner(pos + k)
        part[b] = jnp.dot(hidden[...], full_down[b], preferred_element_type=F32).astype(BF16)

        @pl.when(b // bps != t)
        def _():
            down_copy(b).start()

    down_block(0)
    pumps(DOWN, 3, half)

    def down_step(s, c):
        for w in DOWN:
            for d in (0, 1):
                ring_arrive(w, d, s)
                ring_copy(w, d, s).wait_send()

                @pl.when(s < n - 2)
                def _():
                    ring_copy(w, d, s + 1).start()

        down_block(s + 1)

        @pl.when(s + 1 != n - 1 - s)
        def _():
            down_block(n - 1 - s)

        return c

    lax.fori_loop(half - 1, n - 1, down_step, 0)
    for o in offsets:
        for q in range(bps):
            got = drecv.at[o - 1, q]
            pltpu.make_async_remote_copy(
                src_ref=got, dst_ref=got, send_sem=dn_send.at[0], recv_sem=dn_recv.at[o - 1, q],
                device_id={"tp": peer(o)}, device_id_type=MESH,
            ).wait_recv()
    add_tile(drecv, down_out)
    for o in offsets:
        for q in range(bps):
            down_copy(peer(o) * bps + q).wait_send()


def finish(summed, residual, gain_row):
    floats = summed.astype(F32)
    columns = floats.shape[1]
    squares = lax.psum(jnp.sum(floats * floats, axis=1), "tp")
    factor = lax.rsqrt(squares / (columns * lax.axis_size("tp")) + EPS)
    own_gain = lax.dynamic_slice_in_dim(gain_row, lax.axis_index("tp") * columns, columns)
    return (residual.astype(F32) + floats * factor[:, None] * own_gain).astype(BF16)


def solution(mesh):
    n, nt = mesh.shape["fs"], mesh.shape["tp"]

    def shards(
        tokens, mixer_gain, conv_taps, outer_weight, inner_weight, value_weight, merge_weight,
        merge_gain, channel_gain, gate_weight, up_weight, down_weight, output_gain,
    ):
        length, width = tokens.shape
        blk, channels = outer_weight.shape
        units = gate_weight.shape[1]
        cols = merge_weight.shape[1]
        depth = width * nt
        bps = n // nt
        own_taps = lax.dynamic_slice_in_dim(
            conv_taps, lax.axis_index("tp") * channels, channels, 1
        ).astype(F32)

        def slabs(gain):
            return gain.reshape(nt, 1, width)

        vmem = pl.BlockSpec(memory_space=pltpu.VMEM)
        dma = pltpu.SemaphoreType.DMA
        down, first = pl.pallas_call(
            lambda *refs: layer_kernel(n, nt, *refs),
            out_shape=[jax.ShapeDtypeStruct((length, width), BF16)] * 2,
            in_specs=[vmem] * 12,
            out_specs=[vmem] * 2,
            scratch_shapes=[
                pltpu.VMEM((nt, length, width), BF16),
                pltpu.VMEM((length, depth), BF16),
                pltpu.VMEM((n * blk, channels), BF16),
                pltpu.VMEM((n * blk, channels), BF16),
                pltpu.VMEM((n * blk, channels), BF16),
                pltpu.VMEM((n, channels, cols), BF16),
                pltpu.VMEM((n * blk, units), BF16),
                pltpu.VMEM((n * blk, units), BF16),
                pltpu.VMEM((n, units, cols), BF16),
                pltpu.VMEM((length, channels), F32),
                pltpu.VMEM((length + 8, channels), F32),
                pltpu.VMEM((length, channels), BF16),
                pltpu.VMEM((n, length, cols), BF16),
                pltpu.VMEM((nt - 1, bps, length, cols), BF16),
                pltpu.VMEM((length, width), BF16),
                pltpu.VMEM((nt, length, width), BF16),
                pltpu.VMEM((length, units), BF16),
                pltpu.VMEM((nt - 1, bps, length, cols), BF16),
                dma((2, 8)),
                dma((2, 8, n - 1)),
                dma((nt - 1,)), dma((nt - 1,)),
                dma((nt - 1,)), dma((nt - 1,)),
                dma((nt - 1,)), dma((nt - 1,)),
                dma((n,)), dma((nt - 1, bps)),
            ],
            compiler_params=pltpu.CompilerParams(
                collective_id=0, has_side_effects=True, vmem_limit_bytes=67043328
            ),
        )(
            tokens, slabs(mixer_gain), own_taps, outer_weight, inner_weight, value_weight,
            merge_weight, slabs(merge_gain), slabs(channel_gain), gate_weight, up_weight,
            down_weight,
        )
        return finish(down, first, output_gain)

    return jax.shard_map(
        shards,
        mesh=mesh,
        in_specs=(
            P("fs", "tp"), P(), P(), P("fs", "tp"), P("fs", "tp"), P("fs", "tp"), P("tp", "fs"),
            P(), P(), P("fs", "tp"), P("fs", "tp"), P("tp", "fs"), P(),
        ),
        out_specs=P("fs", "tp"),
        check_vma=False,
    )
```

time: 662 us -> 259 us (0.39)
  waiting for transfers between devices: 574 us -> 0 us
  Pallas kernels: 0 us -> 240 us
  matrix products: 49.7 us -> 0 us
  between operations: 13.6 us -> 0.04 us
  other arithmetic: 16.9 us -> 5.51 us
    all_gather x8 -> x0, waiting for transfers between devices: 445 us -> none  [the longest x1 93.4 us: shards(): lax.all_gather(down_weight, 'fs', axis=1, tiled=True)]
    pallas_call x0 -> x1, Pallas kernels: none -> 240 us  [shards(): pl.pallas_call(lambda *refs: layer_kernel(n, nt, *refs), out_shape=[jax.S...]
    psum x1 -> x0, waiting for transfers between devices: 82.2 us -> none  [shards(): merged = lax.psum(rounded_term(merged_part).astype(jnp.bfloat16), 'tp')]
    dot_general x6 -> x0, matrix products: 49.7 us -> none  [the longest x1 20.8 us: shards(): jnp.dot(hidden, lax.all_gather(down_weight, 'fs', axis=1, tiled=True), pr...]
    reduce_scatter x1 -> x0, waiting for transfers between devices: 42 us -> none  [shards(): lax.psum_scatter(rounded_term(down_part).astype(jnp.bfloat16), 'tp', scat...]
    reduce_sum x4 -> x1, other arithmetic: 13.1 us -> 1.58 us  [finish(): squares = lax.psum(jnp.sum(floats * floats, axis=1), 'tp')]
  transfers between devices with their start and end apart: 10 -> 0, of which waited for: 10 -> 0; matrix products, arithmetic and copies ran while one was open for 6% -> 0% of each run, Pallas kernels for 0% -> 0%
where the time goes in v1:
time: 259 us; the launch traced here: 258 us
  Pallas kernels  240 us (93%)
  blocking collectives  10.8 us (4%)
  other arithmetic  5.51 us (2%)
    pallas_call x1, Pallas kernels, shards(): pl.pallas_call(lambda *refs: layer_kernel(n, nt, *refs), out_shape=[jax.S...  240 us
    psum x1, blocking collectives, finish(): squares = lax.psum(jnp.sum(floats * floats, axis=1), 'tp')  10.8 us

profile of v1, /device:TPU:0, one launch (start us, length us, event | category | flops | bytes accessed | tf_op | source)
XLA Modules:
  0.0 258.2 jit_solution(8627361848141793087)
XLA Ops:
  0.0 1.4 dynamic_slice.7
  1.4 1.3 dynamic-slice_convert_fusion.refs_2_
  2.6 240.4 %shard_map.127 = (bf16[1024,512]{1,0:T(8,128)(2,1)}, bf16[1024,512]{1,0:T(8,128)(2,1)}) custom-call(bf16[1024,512]{1,0:T(8,128)(2,1)} %refs_0_.1, f32[4,1,512]{2,1,0:T(1,128)} %bitcast.3, f32[3,256]{1,0:T(4,128)} %dynamic-slice_convert_fusion.refs_2_, bf16[256,256]{1,0:T(8,128)(2,1)} %refs_3_.1, bf16[256,256]{1,0:T(8,128)(2,1)} %refs_4_.1, ...), custom_call_target="tpu_custom_call" | custom-call | tf_op jit(solution)/shard_map/pallas_call | solution.py:338
  243.1 0.0 copy-start
  243.1 0.0 copy-start.1
  243.1 1.6 fusion
  244.7 10.8 %psum.7 = f32[1024]{0:T(1024)S(1)} all-reduce(f32[1024]{0:T(1024)S(1)} %fusion), channel_id=1, replica_groups=mesh['fs'=8,'tp'=4] {'tp'}, use_global_device_ids=true, to_apply=%region_1.0 | all-reduce | flops 1024 | bytes 8192 | tf_op jit(solution)/shard_map/psum | solution.py:310
  255.5 0.0 copy-done
  255.5 0.0 copy-done.1
  255.5 2.6 %fusion.3 = bf16[1024,512]{1,0:T(8,128)(2,1)} fusion(bf16[1024,512]{1,0:T(8,128)(2,1)S(1)} %copy-done, bf16[1024,512]{1,0:T(8,128)(2,1)} %get-tuple-element.7, f32[512]{0:T(512)S(1)} %copy-done.1, f32[1024]{0:T(1024)S(1)} %add_rsqrt_fusion), kind=kLoop, calls=%fused_computation.5 | loop fusion | flops 3145728 | bytes 3151872 | tf_op jit(solution)/shard_map/convert_element_type | solution.py:313
  (1 shorter events, 0.0 us)
Async XLA Ops:
  243.1 12.4 %copy-start = (bf16[1024,512]{1,0:T(8,128)(2,1)S(1)}, bf16[1024,512]{1,0:T(8,128)(2,1)}, u32[]{:S(2)}) copy-start(bf16[1024,512]{1,0:T(8,128)(2,1)} %get-tuple-element.8) | copy-start | bytes 3145732
  243.1 12.4 %copy-start.1 = (f32[512]{0:T(512)S(1)}, f32[512]{0:T(512)}, u32[]{:S(2)}) copy-start(f32[512]{0:T(512)} %dynamic_slice.7) | copy-start | bytes 6148

commit v2 on v1

--- a/solution.py
+++ b/solution.py
@@ -14,12 +14,13 @@
 
 
 def layer_kernel(
-    n, nt, tokens, mixer_gain, taps, outer_w, inner_w, value_w, merge_w, merge_gain,
-    channel_gain, gate_w, up_w, down_w,
-    down_out, first_out,
+    n, nt, tokens, mixer_gain, conv_taps, outer_w, inner_w, value_w, merge_w, merge_gain,
+    channel_gain, gate_w, up_w, down_w, output_gain,
+    out,
     toks, nrm, full_outer, full_inner, full_value, full_merge, full_gate, full_up, full_down,
-    outer_s, sig, mixed, part, mrecv, msum, merged, hidden, drecv,
+    outer_s, sig, mixed, part, mrecv, msum, merged, hidden, drecv, sq_own, sq_in,
     ring_send, ring_recv, tok_send, tok_recv, rs_send, rs_recv, ag_send, ag_recv, dn_send, dn_recv,
+    sq_send, sq_recv,
 ):
     f, t = lax.axis_index("fs"), lax.axis_index("tp")
     half = n // 2
@@ -44,53 +45,59 @@
     piece_m = channels // 2
     piece_d = down_w.shape[0] // 4
 
-    def own_region(w, d):
+    def own_region(w, h):
         if w in rowed:
-            return rowed[w][0].at[pl.ds(d * (blk // 2), blk // 2)]
+            return rowed[w][0].at[pl.ds(h * (blk // 2), blk // 2)]
         if w == 3:
-            return merge_w.at[pl.ds(d * piece_m, piece_m)]
-        return down_w.at[pl.ds((d * 2 + w - 6) * piece_d, piece_d)]
-
-    def region(w, d, p):
+            return merge_w.at[pl.ds(h * piece_m, piece_m)]
+        return down_w.at[pl.ds((h * 2 + w - 6) * piece_d, piece_d)]
+
+    def region(w, h, p):
         i = owner(p)
         if w in rowed:
-            start = pl.multiple_of(i * blk + d * (blk // 2), blk // 2)
+            start = pl.multiple_of(i * blk + h * (blk // 2), blk // 2)
             return rowed[w][1].at[pl.ds(start, blk // 2)]
         if w == 3:
-            return full_merge.at[i, pl.ds(d * piece_m, piece_m)]
-        return full_down.at[i, pl.ds((d * 2 + w - 6) * piece_d, piece_d)]
-
-    def ring_copy(w, d, s, first=False):
-        p = pos - s if d == 0 else pos + s
-        dst = region(w, d, p)
+            return full_merge.at[i, pl.ds(h * piece_m, piece_m)]
+        return full_down.at[i, pl.ds((h * 2 + w - 6) * piece_d, piece_d)]
+
+    def ring_copy(w, h, d, s, first=False):
+        dst = region(w, h, pos - s if d == 0 else pos + s)
         return pltpu.make_async_remote_copy(
-            src_ref=own_region(w, d) if first else dst,
+            src_ref=own_region(w, h) if first else dst,
             dst_ref=dst,
-            send_sem=ring_send.at[d, w],
-            recv_sem=ring_recv.at[d, w, s],
+            send_sem=ring_send.at[d, h, w],
+            recv_sem=ring_recv.at[d, h, w, s],
             device_id={"fs": right if d == 0 else left},
             device_id_type=MESH,
         )
 
-    def ring_arrive(w, d, s):
-        got = region(w, d, pos - 1 - s if d == 0 else pos + 1 + s)
+    def ring_arrive(w, h, d, s):
+        got = region(w, h, pos - 1 - s if d == 0 else pos + 1 + s)
         pltpu.make_async_remote_copy(
-            src_ref=got, dst_ref=got, send_sem=ring_send.at[d, w],
-            recv_sem=ring_recv.at[d, w, s],
+            src_ref=got, dst_ref=got, send_sem=ring_send.at[d, h, w],
+            recv_sem=ring_recv.at[d, h, w, s],
             device_id={"fs": right if d == 0 else left}, device_id_type=MESH,
         ).wait_recv()
 
+    def pieces(ws):
+        return [(w, h, d) for h in (0, 1) for w in ws for d in (0, 1)]
+
     def ring_open(ws):
-        for w in ws:
-            for d in (0, 1):
-                ring_copy(w, d, 0, True).start()
-
-    def pump(ws, s):
-        for w in ws:
-            for d in (0, 1):
-                ring_arrive(w, d, s - 1)
-                ring_copy(w, d, s - 1).wait_send()
-                ring_copy(w, d, s).start()
+        for w, h, d in pieces(ws):
+            ring_copy(w, h, d, 0, True).start()
+
+    def pump(ws, s, last=False):
+        for w, h, d in pieces(ws):
+            if last and h != d:
+                continue
+            ring_arrive(w, h, d, s - 1)
+            ring_copy(w, h, d, s - 1).wait_send()
+            ring_copy(w, h, d, s).start()
+        for w, h, d in pieces(ws):
+            if last and h != d:
+                ring_arrive(w, h, d, s - 1)
+                ring_copy(w, h, d, s - 1).wait_send()
 
     def pumps(ws, low, high):
         lax.fori_loop(low, high, lambda s, c: (pump(ws, s), c)[1], 0)
@@ -98,8 +105,8 @@
     def ring_close(ws):
         for w in ws:
             for d in (0, 1):
-                ring_arrive(w, d, n - 2)
-                ring_copy(w, d, n - 2).wait_send()
+                ring_arrive(w, d, d, half - 1)
+                ring_copy(w, d, d, half - 1).wait_send()
 
     def peer(o):
         return lax.rem(t + o, nt)
@@ -111,6 +118,34 @@
         )
 
     offsets = range(1, nt)
+    partner = t + 1 - 2 * lax.rem(t, 2)
+    strides = range(2, nt, 2)
+
+    def hop(src, dst, send, recv, i, to):
+        return pltpu.make_async_remote_copy(
+            src_ref=src, dst_ref=dst, send_sem=send.at[i], recv_sem=recv.at[i],
+            device_id={"tp": to}, device_id_type=MESH,
+        )
+
+    def gather_open(own, held, send, recv):
+        for o in strides:
+            hop(own, held.at[t], send, recv, o - 1, peer(o)).start()
+        hop(own, held.at[t], send, recv, 0, partner).start()
+
+    def gather_relay(own, held, send, recv):
+        for o in strides:
+            slab = held.at[peer(nt - o)]
+            hop(own, slab, send, recv, o - 1, peer(o)).wait()
+            hop(slab, slab, send, recv, o, partner).start()
+
+    def gather_close(own, held, send, recv):
+        hop(own, held.at[partner], send, recv, 0, partner).wait()
+        for o in strides:
+            slab = held.at[lax.rem(partner + nt - o, nt)]
+            hop(held.at[peer(nt - o)], slab, send, recv, o, partner).wait()
+
+    tok_args = (tokens, toks, tok_send, tok_recv)
+    sum_args = (msum, merged, ag_send, ag_recv)
 
     barrier = pltpu.get_barrier_semaphore()
     for to in ({"fs": left}, {"fs": right}) + tuple({"tp": peer(o)} for o in offsets):
@@ -118,8 +153,7 @@
     pl.semaphore_wait(barrier, 2 + nt - 1)
 
     ring_open(MIX)
-    for o in offsets:
-        slab_copy(tokens, toks.at[t], tok_send, tok_recv, o).start()
+    gather_open(*tok_args)
 
     own_rows = pl.ds(pl.multiple_of(f * blk, blk), blk)
     for source, full in rowed.values():
@@ -129,11 +163,12 @@
     toks[t] = tokens[...]
     sig[pl.ds(0, 8), :] = jnp.zeros((8, channels), F32)
 
-    pumps(MIX, 1, n - 1)
+    pumps(MIX, 1, half - 1)
+    gather_relay(*tok_args)
+    pump(MIX, half - 1, True)
     ring_open(FEED)
-    for o in offsets:
-        slab = toks.at[lax.rem(t - o + nt, nt)]
-        slab_copy(tokens, slab, tok_send, tok_recv, o).wait()
+    gather_close(*tok_args)
+    taps = conv_taps[:, pl.ds(pl.multiple_of(t * channels, channels), channels)].astype(F32)
 
     def rows_of(i):
         return pl.ds(pl.multiple_of(i * tile, tile), tile)
@@ -187,8 +222,7 @@
 
     for o in offsets:
         slab_copy(part_slab(peer(o)), mrecv.at[o - 1], rs_send, rs_recv, o).start()
-    cut = (2 * (n - 2) + 2) // 3
-    pumps(FEED, 1, cut + 1)
+    pumps(FEED, 1, half - 1)
     for o in offsets:
         slab_copy(part_slab(peer(o)), mrecv.at[o - 1], rs_send, rs_recv, o).wait()
 
@@ -205,14 +239,12 @@
         lax.fori_loop(0, tiles, body, 0)
 
     add_tile(mrecv, msum)
-    for o in offsets:
-        slab_copy(msum, merged.at[t], ag_send, ag_recv, o).start()
+    gather_open(*sum_args)
     merged[t] = msum[...]
-    pumps(FEED, cut + 1, n - 1)
+    pump(FEED, half - 1, True)
     ring_open(DOWN)
-    for o in offsets:
-        slab = merged.at[lax.rem(t - o + nt, nt)]
-        slab_copy(msum, slab, ag_send, ag_recv, o).wait()
+    gather_relay(*sum_args)
+    gather_close(*sum_args)
 
     def first_tile(i, c):
         rows = rows_of(i)
@@ -235,7 +267,6 @@
         return c
 
     lax.fori_loop(0, tiles, first_tile, 0)
-    first_out[...] = toks[t]
     ring_close(FEED)
 
     def feed_tile(i, c):
@@ -246,10 +277,9 @@
         hidden[rows, :] = (gate / (1.0 + jnp.exp(-gate)) * upward).astype(BF16)
         return c
 
-    lax.fori_loop(0, tiles // 2, feed_tile, 0)
+    lax.fori_loop(0, tiles * 3 // 4, feed_tile, 0)
     pump(DOWN, 1)
-    lax.fori_loop(tiles // 2, tiles, feed_tile, 0)
-    pump(DOWN, 2)
+    lax.fori_loop(tiles * 3 // 4, tiles, feed_tile, 0)
 
     def down_copy(b):
         j = b // bps
@@ -269,28 +299,21 @@
         def _():
             down_copy(b).start()
 
+    def down_pair(s):
+        lax.fori_loop(0, 2, lambda i, c: (down_block(s - 2 * s * i), c)[1], 0)
+
+    def down_step(s, c):
+        pump(DOWN, s)
+        down_pair(s)
+        return c
+
     down_block(0)
-    pumps(DOWN, 3, half)
-
-    def down_step(s, c):
-        for w in DOWN:
-            for d in (0, 1):
-                ring_arrive(w, d, s)
-                ring_copy(w, d, s).wait_send()
-
-                @pl.when(s < n - 2)
-                def _():
-                    ring_copy(w, d, s + 1).start()
-
-        down_block(s + 1)
-
-        @pl.when(s + 1 != n - 1 - s)
-        def _():
-            down_block(n - 1 - s)
-
-        return c
-
-    lax.fori_loop(half - 1, n - 1, down_step, 0)
+    down_pair(1)
+    lax.fori_loop(2, half - 1, down_step, 0)
+    pump(DOWN, half - 1, True)
+    down_pair(half - 1)
+    ring_close(DOWN)
+    down_block(half)
     for o in offsets:
         for q in range(bps):
             got = drecv.at[o - 1, q]
@@ -298,19 +321,37 @@
                 src_ref=got, dst_ref=got, send_sem=dn_send.at[0], recv_sem=dn_recv.at[o - 1, q],
                 device_id={"tp": peer(o)}, device_id_type=MESH,
             ).wait_recv()
-    add_tile(drecv, down_out)
+    add_tile(drecv, msum)
+
+    def square_tile(i, c):
+        rows = rows_of(i)
+        x = msum[rows, :].astype(F32)
+        sq_own[:, rows] = lax.dot_general(
+            jnp.ones((8, width), F32), x * x, (((1,), (1,)), ((), ())),
+            precision=lax.Precision.HIGHEST, preferred_element_type=F32,
+        )
+        return c
+
+    lax.fori_loop(0, tiles, square_tile, 0)
+    for o in offsets:
+        slab_copy(sq_own, sq_in.at[o - 1], sq_send, sq_recv, o).start()
     for o in offsets:
         for q in range(bps):
             down_copy(peer(o) * bps + q).wait_send()
-
-
-def finish(summed, residual, gain_row):
-    floats = summed.astype(F32)
-    columns = floats.shape[1]
-    squares = lax.psum(jnp.sum(floats * floats, axis=1), "tp")
-    factor = lax.rsqrt(squares / (columns * lax.axis_size("tp")) + EPS)
-    own_gain = lax.dynamic_slice_in_dim(gain_row, lax.axis_index("tp") * columns, columns)
-    return (residual.astype(F32) + floats * factor[:, None] * own_gain).astype(BF16)
+    for o in offsets:
+        slab_copy(sq_own, sq_in.at[o - 1], sq_send, sq_recv, o).wait()
+
+    def last_tile(i, c):
+        rows = rows_of(i)
+        squares = sq_own[:, rows]
+        for o in offsets:
+            squares += sq_in[o - 1, :, rows]
+        factor = lax.rsqrt(jnp.transpose(squares)[:, 0:1] / depth + EPS)
+        y = toks[t, rows, :].astype(F32) + msum[rows, :].astype(F32) * factor * output_gain[t]
+        out[rows, :] = y.astype(BF16)
+        return c
+
+    lax.fori_loop(0, tiles, last_tile, 0)
 
 
 def solution(mesh):
@@ -326,20 +367,16 @@
         cols = merge_weight.shape[1]
         depth = width * nt
         bps = n // nt
-        own_taps = lax.dynamic_slice_in_dim(
-            conv_taps, lax.axis_index("tp") * channels, channels, 1
-        ).astype(F32)
-
         def slabs(gain):
             return gain.reshape(nt, 1, width)
 
         vmem = pl.BlockSpec(memory_space=pltpu.VMEM)
         dma = pltpu.SemaphoreType.DMA
-        down, first = pl.pallas_call(
+        return pl.pallas_call(
             lambda *refs: layer_kernel(n, nt, *refs),
-            out_shape=[jax.ShapeDtypeStruct((length, width), BF16)] * 2,
-            in_specs=[vmem] * 12,
-            out_specs=[vmem] * 2,
+            out_shape=jax.ShapeDtypeStruct((length, width), BF16),
+            in_specs=[vmem] * 13,
+            out_specs=vmem,
             scratch_shapes=[
                 pltpu.VMEM((nt, length, width), BF16),
                 pltpu.VMEM((length, depth), BF16),
@@ -359,22 +396,24 @@
                 pltpu.VMEM((nt, length, width), BF16),
                 pltpu.VMEM((length, units), BF16),
                 pltpu.VMEM((nt - 1, bps, length, cols), BF16),
-                dma((2, 8)),
-                dma((2, 8, n - 1)),
+                pltpu.VMEM((8, length), F32),
+                pltpu.VMEM((nt - 1, 8, length), F32),
+                dma((2, 2, 8)),
+                dma((2, 2, 8, n // 2)),
                 dma((nt - 1,)), dma((nt - 1,)),
                 dma((nt - 1,)), dma((nt - 1,)),
                 dma((nt - 1,)), dma((nt - 1,)),
                 dma((n,)), dma((nt - 1, bps)),
+                dma((nt - 1,)), dma((nt - 1,)),
             ],
             compiler_params=pltpu.CompilerParams(
                 collective_id=0, has_side_effects=True, vmem_limit_bytes=67043328
             ),
         )(
-            tokens, slabs(mixer_gain), own_taps, outer_weight, inner_weight, value_weight,
+            tokens, slabs(mixer_gain), conv_taps, outer_weight, inner_weight, value_weight,
             merge_weight, slabs(merge_gain), slabs(channel_gain), gate_weight, up_weight,
-            down_weight,
-        )
-        return finish(down, first, output_gain)
+            down_weight, slabs(output_gain),
+        )
 
     return jax.shard_map(
         shards,

time: 259 us -> 249 us (0.961)
  blocking collectives: 10.8 us -> 0 us
  Pallas kernels: 240 us -> 247 us
  other arithmetic: 5.51 us -> 0 us
    psum x1 -> x0, blocking collectives: 10.8 us -> none  [finish(): squares = lax.psum(jnp.sum(floats * floats, axis=1), 'tp')]
    pallas_call x1, Pallas kernels: 240 us -> 247 us  [shards(): pl.pallas_call(lambda *refs: layer_kernel(n, nt, *refs), out_shape=jax.Sh...]
    convert_element_type x2 -> x0, other arithmetic: 3.92 us -> none  [the longest x1 2.64 us: finish(): (residual.astype(F32) + floats * factor[:, None] * own_gain).astype(BF16)]
where the time goes in v2:
time: 249 us
  Pallas kernels  247 us (99%)
    pallas_call x1, Pallas kernels, shards(): pl.pallas_call(lambda *refs: layer_kernel(n, nt, *refs), out_shape=jax.Sh...  247 us

profile of v2, /device:TPU:0, one launch (start us, length us, event | category | flops | bytes accessed | tf_op | source)
XLA Modules:
  0.0 249.1 jit_solution(16399827626692187500)
XLA Ops:
  0.0 246.8 %shard_map.127 = bf16[1024,512]{1,0:T(8,128)(2,1)} custom-call(bf16[1024,512]{1,0:T(8,128)(2,1)} %refs_0_.1, f32[4,1,512]{2,1,0:T(1,128)} %bitcast.4, bf16[3,1024]{1,0:T(4,128)(2,1)} %refs_2_.1, bf16[256,256]{1,0:T(8,128)(2,1)} %refs_3_.1, bf16[256,256]{1,0:T(8,128)(2,1)} %refs_4_.1, bf16[256,256]{1,0:T(8,128)(2,1)} %refs_5_.1, bf16[256,256]{1,0:T(8,128)(2,1)} %refs_6_.1, ...), custom_call_target="tpu_custom_call" | custom-call | tf_op jit(solution)/shard_map/pallas_call | solution.py:375
  246.8 2.3 copy.15

commit v3 on v2

--- a/solution.py
+++ b/solution.py
@@ -81,7 +81,7 @@
         ).wait_recv()
 
     def pieces(ws):
-        return [(w, h, d) for h in (0, 1) for w in ws for d in (0, 1)]
+        return [(w, (i + d) % 2, d) for i in (0, 1) for w in ws for d in (0, 1)]
 
     def ring_open(ws):
         for w, h, d in pieces(ws):

time: 249 us -> 249 us (level)
  no operation moved by 1% of the time
where the time goes in v3:
time: 249 us
  Pallas kernels  247 us (99%)
    pallas_call x1, Pallas kernels, shards(): pl.pallas_call(lambda *refs: layer_kernel(n, nt, *refs), out_shape=jax.Sh...  247 us

profile of v3, /device:TPU:0, one launch (start us, length us, event | category | flops | bytes accessed | tf_op | source)
XLA Modules:
  0.0 249.0 jit_solution(2010159558894322122)
XLA Ops:
  0.0 246.8 %shard_map.127 = bf16[1024,512]{1,0:T(8,128)(2,1)} custom-call(bf16[1024,512]{1,0:T(8,128)(2,1)} %refs_0_.1, f32[4,1,512]{2,1,0:T(1,128)} %bitcast.4, bf16[3,1024]{1,0:T(4,128)(2,1)} %refs_2_.1, bf16[256,256]{1,0:T(8,128)(2,1)} %refs_3_.1, bf16[256,256]{1,0:T(8,128)(2,1)} %refs_4_.1, bf16[256,256]{1,0:T(8,128)(2,1)} %refs_5_.1, bf16[256,256]{1,0:T(8,128)(2,1)} %refs_6_.1, ...), custom_call_target="tpu_custom_call" | custom-call | tf_op jit(solution)/shard_map/pallas_call | solution.py:375
  246.8 2.3 copy.15
